TPU v7x, 32 devices: a whole 2x2x4 slice. The times are simulated.
32 devices in a mesh: rep: 4 (over z), fs: 4 (over y, x), tp: 2 (over core).
Axes of the slice: x: 2, y: 2, z: 4, core: 2. Of those that a mesh axis runs over, the one named last changes fastest.
Arguments:
- tokens_in: bfloat16 [8192, 2048], P(('rep', 'fs', 'tp')), may hold values from -6 to 6
- norm_gain: float32 [2048], replicated, may hold values from 0.1 to 1.9
- gate_weight: bfloat16 [2048, 3072], P(None, ('fs', 'tp')), may hold values from -0.125 to 0.125
- up_weight: bfloat16 [2048, 3072], P(None, ('fs', 'tp')), may hold values from -0.125 to 0.125
- down_weight: bfloat16 [3072, 2048], P(('fs', 'tp')), may hold values from -0.109375 to 0.109375
- out_grad: bfloat16 [8192, 2048], P(('rep', 'fs', 'tp')), may hold values from -6 to 6
Outputs:
- grad_in: bfloat16 [8192, 2048], P(('rep', 'fs', 'tp'))
- grad_gain: float32 [2048], replicated
- grad_gate: float32 [2048, 3072], P(None, ('fs', 'tp'))
- grad_up: float32 [2048, 3072], P(None, ('fs', 'tp'))
- grad_down: float32 [3072, 2048], P(('fs', 'tp'))
All inputs are finite; a program needn't handle non-finite values.
Results may differ from a plain program's by a relative error of at most 0.014.
Values may be sent and summed in bfloat16 or wider, within the bound.
A program may use at most 192 MiB of HBM per device.

v0:
```python
import jax
import jax.numpy as jnp
from jax import lax
from jax.sharding import PartitionSpec as P

norm_eps = 1e-06


def shards(tokens_in, norm_gain, gate_weight, up_weight, down_weight, out_grad):
    row_count = tokens_in.shape[0]
    total_tokens = row_count * lax.axis_size("rep") * lax.axis_size("fs") * lax.axis_size("tp")
    factor = float(total_tokens) ** (-0.5)
    whole_in, whole_grad = (
        lax.all_gather(tokens_in, ("fs", "tp"), axis=0, tiled=True),
        lax.all_gather(out_grad, ("fs", "tp"), axis=0, tiled=True),
    )
    floats = whole_in.astype(jnp.float32)
    inverse = lax.rsqrt(jnp.mean(floats * floats, axis=-1, keepdims=True) + norm_eps)
    unit_rows = floats * inverse
    normed = (unit_rows * norm_gain).astype(jnp.bfloat16)
    gate_pre = jnp.dot(normed, gate_weight, preferred_element_type=jnp.float32)
    up_pre = jnp.dot(normed, up_weight, preferred_element_type=jnp.float32)
    sigma = jax.nn.sigmoid(gate_pre)
    active = gate_pre * sigma
    hidden = (active * up_pre).astype(jnp.bfloat16)
    grad_hidden = 0.5 * jnp.dot(whole_grad, down_weight.T, preferred_element_type=jnp.float32)
    grad_gate_pre = (grad_hidden * up_pre * sigma * (1.0 + gate_pre * (1.0 - sigma))).astype(
        jnp.bfloat16
    )
    grad_up_pre = (grad_hidden * active).astype(jnp.bfloat16)
    result = jnp.dot(grad_gate_pre, gate_weight.T, preferred_element_type=jnp.float32)
    grad_normed = lax.psum_scatter(
        (result + jnp.dot(grad_up_pre, up_weight.T, preferred_element_type=jnp.float32)).astype(
            jnp.bfloat16
        ),
        ("fs", "tp"),
        scatter_dimension=0,
        tiled=True,
    ).astype(jnp.float32)
    local_gate = jnp.dot(normed.T, grad_gate_pre, preferred_element_type=jnp.float32)
    local_up = jnp.dot(normed.T, grad_up_pre, preferred_element_type=jnp.float32)
    local_down = jnp.dot(hidden.T, whole_grad, preferred_element_type=jnp.float32)
    summed_gate = lax.psum(local_gate.astype(jnp.bfloat16), "rep").astype(jnp.float32)
    summed_up = lax.psum(local_up.astype(jnp.bfloat16), "rep").astype(jnp.float32)
    summed_down = lax.psum(local_down.astype(jnp.bfloat16), "rep").astype(jnp.float32)
    grad_gate = summed_gate * factor
    grad_up = summed_up * factor
    grad_down = summed_down * (0.5 * factor)
    position = lax.axis_index("fs") * lax.axis_size("tp") + lax.axis_index("tp")
    own_unit = lax.dynamic_slice_in_dim(unit_rows, position * row_count, row_count, 0)
    own_inverse = lax.dynamic_slice_in_dim(inverse, position * row_count, row_count, 0)
    gain_local = jnp.sum(grad_normed * own_unit, axis=0)
    gain_partial = lax.psum(gain_local, ("fs", "tp"))
    grad_gain = lax.psum(gain_partial, "rep")
    scaled = grad_normed * norm_gain
    grad_in = (
        out_grad.astype(jnp.float32)
        + own_inverse * scaled
        - own_unit * own_inverse * jnp.mean(scaled * own_unit, axis=-1, keepdims=True)
    )
    return (grad_in.astype(jnp.bfloat16), grad_gain, grad_gate, grad_up, grad_down)


def solution(mesh):
    in_specs = (
        P(("rep", "fs", "tp"), None),
        P(),
        P(None, ("fs", "tp")),
        P(None, ("fs", "tp")),
        P(("fs", "tp"), None),
        P(("rep", "fs", "tp"), None),
    )
    out_specs = (
        P(("rep", "fs", "tp"), None),
        P(),
        P(None, ("fs", "tp")),
        P(None, ("fs", "tp")),
        P(("fs", "tp"), None),
    )
    return jax.shard_map(shards, mesh=mesh, in_specs=in_specs, out_specs=out_specs, check_vma=False)
```

profile of v0, /device:TPU:0, one launch (start us, length us, event | category | flops | bytes accessed | tf_op | source)
XLA Modules:
  0.0 437.0 jit_solution(11326514007255932176)
XLA Ops:
  7.2 0.0 copy-start
  7.2 0.0 all-gather.3.cloned.1.call-start
  7.2 0.0 copy-start.3
  7.2 0.7 all-gather.3.cloned.1.call-update
  7.9 0.0 all-gather.5.cloned.1.call-start
  8.0 0.7 all-gather.5.cloned.1.call-update
  8.7 0.0 copy-start.9
  8.7 0.0 all-reduce.3.cloned.1.call-start
  8.7 58.2 %all-gather.3.cloned.1.call-done = bf16[2048,2048]{1,0:T(8,128)(2,1)} async-done(((bf16[256,2048]{1,0:T(8,128)(2,1)}), bf16[2048,2048]{1,0:T(8,128)(2,1)}) %all-gather.3.cloned.1.call-update) | async-done | bytes 8388624 | tf_op jit(solution)/shard_map/all_gather | solution.py:14
  66.9 5.2 %fusion = f32[2048]{0:T(1024)S(1)} fusion(bf16[2048,2048]{1,0:T(8,128)(2,1)} %all-gather.3.cloned.1.call-done), kind=kLoop, calls=%fused_computation.2 | loop fusion | flops 12580864 | bytes 8396800 | tf_op jit(solution)/shard_map/reduce_sum | solution.py:18
  72.1 0.0 copy-done.3
  72.1 0.0 copy-done.9
  72.2 0.5 copy-done.1
  72.7 6.4 %fusion.12 = f32[2048,384]{1,0:T(8,128)} fusion(bf16[2048,384]{1,0:T(8,128)(2,1)S(1)} %copy-done.3, f32[2048]{0:T(1024)S(1)} %copy-done.9, f32[2048]{0:T(1024)S(1)} %add_rsqrt_fusion, bf16[2048,2048]{1,0:T(8,128)(2,1)S(1)} %copy-done.1), kind=kOutput, calls=%fused_computation.30 | convolution fusion | flops 3238002688 | bytes 13123584 | tf_op jit(solution)/shard_map/dot_general | solution.py:22
  79.0 0.0 copy-done
  79.0 6.3 %fusion.11 = f32[2048,384]{1,0:T(8,128)} fusion(bf16[2048,384]{1,0:T(8,128)(2,1)S(1)} %copy-done, f32[2048]{0:T(1024)S(1)} %copy-done.9, f32[2048]{0:T(1024)S(1)} %add_rsqrt_fusion, bf16[2048,2048]{1,0:T(8,128)(2,1)S(1)} %copy-done.1), kind=kOutput, calls=%fused_computation.29 | convolution fusion | flops 3238002688 | bytes 13123584 | tf_op jit(solution)/shard_map/dot_general | solution.py:21
  85.4 37.7 %all-gather.5.cloned.1.call-done = bf16[2048,2048]{1,0:T(8,128)(2,1)} async-done(((bf16[256,2048]{1,0:T(8,128)(2,1)}), bf16[2048,2048]{1,0:T(8,128)(2,1)}) %all-gather.5.cloned.1.call-update) | async-done | bytes 8388624 | tf_op jit(solution)/shard_map/all_gather | solution.py:15
  123.1 10.3 %convolution_convert_fusion = bf16[384,2048]{1,0:T(8,128)(2,1)} fusion(bf16[2048,2048]{1,0:T(8,128)(2,1)} %all-gather.5.cloned.1.call-done, f32[2048,384]{1,0:T(8,128)} %fusion.12, f32[2048,384]{1,0:T(8,128)} %fusion.11), kind=kOutput, calls=%fused_computation.14 | convolution fusion | flops 3226730496 | bytes 16252928 | tf_op jit(solution)/shard_map/dot_general | solution.py:42
  133.4 0.0 copy-done.10
  133.4 0.0 copy-done.11
  133.4 0.0 copy-done.12
  133.4 0.0 slice-start.1
  133.4 7.5 %multiply_convert_fusion.2 = (bf16[2048,384]{1,0:T(8,128)(2,1)S(1)}, bf16[2048,384]{1,0:T(8,128)(2,1)S(1)}) fusion(f32[2048,384]{1,0:T(8,128)} %fusion.11, f32[2048,384]{1,0:T(8,128)S(1)} %copy-done.12, bf16[2048,2048]{1,0:T(8,128)(2,1)S(1)} %copy-done.10, bf16[384,2048]{1,0:T(8,128)(2,1)S(1)} %copy-done.11), kind=kOutput, calls=%fused_computation.9 | convolution fusion | flops 3232235520 | bytes 19398656 | tf_op jit(solution)/shard_map/dot_general | solution.py:26
  140.9 0.0 copy-start.6
  140.9 0.0 copy-start.8
  140.9 0.0 slice-done
  141.0 0.0 slice-done.1
  141.0 6.1 %convolution_convert_fusion.1 = bf16[2048,384]{1,0:T(8,128)(2,1)} fusion(bf16[2048,384]{1,0:T(8,128)(2,1)S(1)} %get-tuple-element.10, f32[2048]{0:T(1024)S(1)} %copy-done.9, f32[2048]{0:T(1024)S(1)} %add_rsqrt_fusion, bf16[2048,2048]{1,0:T(8,128)(2,1)S(1)} %bitcast.12), kind=kOutput, calls=%fused_computation.15 | convolution fusion | flops 3238789120 | bytes 11550720 | tf_op jit(solution)/shard_map/dot_general | solution.py:41
  147.1 0.0 copy-done.6
  147.1 0.0 copy-done.8
  147.1 6.0 %convolution_convert_fusion.2 = bf16[2048,384]{1,0:T(8,128)(2,1)} fusion(bf16[2048,384]{1,0:T(8,128)(2,1)S(1)} %get-tuple-element.11, f32[2048]{0:T(1024)S(1)} %copy-done.9, f32[2048]{0:T(1024)S(1)} %add_rsqrt_fusion, bf16[2048,2048]{1,0:T(8,128)(2,1)S(1)} %bitcast.12), kind=kOutput, calls=%fused_computation.16 | convolution fusion | flops 3238789120 | bytes 11550720 | tf_op jit(solution)/shard_map/dot_general | solution.py:40
  153.1 0.0 all-reduce.3.cloned.1.call-update
  153.1 0.3 reduce-scatter.2.cloned.1.call-start
  153.4 0.0 copy-start.7
  153.4 10.1 %fusion.13 = f32[2048,2048]{1,0:T(8,128)} fusion(bf16[2048,384]{1,0:T(8,128)(2,1)} %copy-done.8, bf16[2048,384]{1,0:T(8,128)(2,1)S(1)} %copy-done), kind=kOutput, calls=%fused_computation.31 | convolution fusion | flops 3221225472 | bytes 19922944 | tf_op jit(solution)/shard_map/dot_general | solution.py:31
  163.5 0.0 copy-done.7
  163.5 10.3 %add_convert_fusion = bf16[2048,2048]{1,0:T(8,128)(2,1)} fusion(f32[2048,2048]{1,0:T(8,128)} %fusion.13, bf16[2048,384]{1,0:T(8,128)(2,1)S(1)} %copy-done.7, bf16[2048,384]{1,0:T(8,128)(2,1)S(1)} %copy-done.3), kind=kOutput, calls=%fused_computation.3 | convolution fusion | flops 3229614080 | bytes 28311552 | tf_op jit(solution)/shard_map/dot_general | solution.py:33
  173.8 0.0 reduce-scatter.2.cloned.1.call-update
  173.9 0.1 dynamic-slice.3
  174.0 10.4 %convert_multiply_fusion = f32[2048,2048]{1,0:T(8,128)} fusion(bf16[2048,2048]{1,0:T(8,128)(2,1)} %all-gather.3.cloned.1.call-done, f32[2048]{0:T(1024)S(1)} %add_rsqrt_fusion), kind=kLoop, calls=%fused_computation | loop fusion | flops 8388608 | bytes 25174016 | tf_op jit(solution)/shard_map/mul | solution.py:19
  184.3 141.0 %all-reduce.3.cloned.1.call-done = (bf16[2048,384]{1,0:T(8,128)(2,1)}, bf16[2048,384]{1,0:T(8,128)(2,1)}, bf16[384,2048]{1,0:T(8,128)(2,1)}) async-done(((bf16[2048,384]{1,0:T(8,128)(2,1)}, bf16[2048,384]{1,0:T(8,128)(2,1)}, bf16[384,2048]{1,0:T(8,128)(2,1)}), (bf16[2048,384]{1,0:T(8,128)(2,1)}, bf16[2048,384]{1,0:T(8,128)(2,1)}, bf16[384,2048]{1,0:T(8,128)(2,1)})) %all-reduce.3.cloned.1.call-update) | async-done | bytes 4718608 | tf_op jit(solution)/shard_map/psum | solution.py:43
  325.3 3.6 convert_multiply_fusion.2
  328.9 3.3 convert_multiply_fusion.3
  332.2 66.9 %reduce-scatter.2.cloned.1.call-done = bf16[256,2048]{1,0:T(8,128)(2,1)} async-done(((bf16[2048,2048]{1,0:T(8,128)(2,1)}), bf16[256,2048]{1,0:T(8,128)(2,1)}) %reduce-scatter.2.cloned.1.call-update) | async-done | bytes 1048592 | tf_op jit(solution)/shard_map/reduce_scatter | solution.py:32
  399.1 2.6 fusion.8
  401.7 12.8 %psum.35 = f32[2048]{0:T(1024)S(1)} all-reduce(f32[2048]{0:T(1024)S(1)} %get-tuple-element.5), channel_id=1, replica_groups=mesh['rep'=4,'fs'=4,'tp'=2] {'fs','tp'}, use_global_device_ids=true, to_apply=%region_4.0 | all-reduce | flops 2048 | bytes 16384 | tf_op jit(solution)/shard_map/psum | solution.py:53
  414.4 12.4 %psum.36 = f32[2048]{0:T(1024)} all-reduce(f32[2048]{0:T(1024)S(1)} %psum.35), channel_id=1, replica_groups=mesh['rep'=4,'fs'=4,'tp'=2] {'rep'}, use_global_device_ids=true, to_apply=%region_5.0 | all-reduce | flops 2048 | bytes 16384 | tf_op jit(solution)/shard_map/psum | solution.py:54
  426.9 3.6 fusion.6
  (14 shorter events, 0.0 us)
Async XLA Ops:
  7.2 71.8 %copy-start = (bf16[2048,384]{1,0:T(8,128)(2,1)S(1)}, bf16[2048,384]{1,0:T(8,128)(2,1)}, u32[]{:S(2)}) copy-start(bf16[2048,384]{1,0:T(8,128)(2,1)} %param.8) | copy-start | bytes 4718596
  7.2 59.7 %all-gather.3.cloned.1.call-start = ((), (), s32[]{:S(2)}) async-start(), calls=%async_computation.1 | async-start | bytes 9437184 | tf_op jit(solution)/shard_map/all_gather | solution.py:14
  7.2 64.9 %copy-start.3 = (bf16[2048,384]{1,0:T(8,128)(2,1)S(1)}, bf16[2048,384]{1,0:T(8,128)(2,1)}, u32[]{:S(2)}) copy-start(bf16[2048,384]{1,0:T(8,128)(2,1)} %param.9) | copy-start | bytes 4718596
  7.9 115.2 %all-gather.5.cloned.1.call-start = ((), (), s32[]{:S(2)}) async-start(), calls=%async_computation.2 | async-start | bytes 9437184 | tf_op jit(solution)/shard_map/all_gather | solution.py:15
  8.7 63.5 %copy-start.9 = (f32[2048]{0:T(1024)S(1)}, f32[2048]{0:T(1024)}, u32[]{:S(2)}) copy-start(f32[2048]{0:T(1024)} %param.7) | copy-start | bytes 24580
  8.7 316.6 %all-reduce.3.cloned.1.call-start = ((), (), s32[]{:S(2)}) async-start(), calls=%async_computation.4 | async-start | bytes 9437184 | tf_op jit(solution)/shard_map/psum | solution.py:43
  66.9 5.8 %copy-start.1 = (bf16[2048,2048]{1,0:T(8,128)(2,1)S(1)}, bf16[2048,2048]{1,0:T(8,128)(2,1)}, u32[]{:S(2)}) copy-start(bf16[2048,2048]{1,0:T(8,128)(2,1)} %all-gather.3.cloned.1.call-done) | copy-start | bytes 25165828
  123.1 10.4 %copy-start.10 = (bf16[2048,2048]{1,0:T(8,128)(2,1)S(1)}, bf16[2048,2048]{1,0:T(8,128)(2,1)}, u32[]{:S(2)}) copy-start(bf16[2048,2048]{1,0:T(8,128)(2,1)} %all-gather.5.cloned.1.call-done) | copy-start | bytes 25165828
  123.1 10.4 %copy-start.11 = (bf16[384,2048]{1,0:T(8,128)(2,1)S(1)}, bf16[384,2048]{1,0:T(8,128)(2,1)}, u32[]{:S(2)}) copy-start(bf16[384,2048]{1,0:T(8,128)(2,1)} %param.10) | copy-start | bytes 4718596
  123.1 10.4 %copy-start.12 = (f32[2048,384]{1,0:T(8,128)S(1)}, f32[2048,384]{1,0:T(8,128)}, u32[]{:S(2)}) copy-start(f32[2048,384]{1,0:T(8,128)} %fusion.12) | copy-start | bytes 9437188
  123.1 17.9 %slice-start = ((s8[8388608]{0:T(1024)(128)(4,1)}), s8[4194304]{0:T(1024)(128)(4,1)S(1)}, s32[]{:S(2)}) async-start(s8[8388608]{0:T(1024)(128)(4,1)} %bitcast.11), calls=%async_computation.5 | async-start | bytes 8388608
  133.4 7.5 %slice-start.1 = ((s8[8388608]{0:T(1024)(128)(4,1)}), s8[4194304]{0:T(1024)(128)(4,1)S(1)}, s32[]{:S(2)}) async-start(s8[8388608]{0:T(1024)(128)(4,1)} %bitcast.11), calls=%async_computation.6 | async-start | bytes 8388608
  140.9 6.1 %copy-start.6 = (bf16[2048,384]{1,0:T(8,128)(2,1)}, bf16[2048,384]{1,0:T(8,128)(2,1)S(1)}, u32[]{:S(2)}) copy-start(bf16[2048,384]{1,0:T(8,128)(2,1)S(1)} %get-tuple-element.10) | copy-start | bytes 4718596
  140.9 6.1 %copy-start.8 = (bf16[2048,384]{1,0:T(8,128)(2,1)}, bf16[2048,384]{1,0:T(8,128)(2,1)S(1)}, u32[]{:S(2)}) copy-start(bf16[2048,384]{1,0:T(8,128)(2,1)S(1)} %get-tuple-element.11) | copy-start | bytes 4718596
  153.1 246.0 %reduce-scatter.2.cloned.1.call-start = ((), (), s32[]{:S(2)}) async-start(), calls=%async_computation.3 | async-start | bytes 9437184 | tf_op jit(solution)/shard_map/reduce_scatter | solution.py:32
  153.4 10.1 %copy-start.7 = (bf16[2048,384]{1,0:T(8,128)(2,1)S(1)}, bf16[2048,384]{1,0:T(8,128)(2,1)}, u32[]{:S(2)}) copy-start(bf16[2048,384]{1,0:T(8,128)(2,1)} %copy-done.6) | copy-start | bytes 4718596
  325.3 3.6 copy-start.4
  325.3 3.6 copy-start.5
  332.2 94.7 %copy-start.2 = (bf16[256,2048]{1,0:T(8,128)(2,1)S(1)}, bf16[256,2048]{1,0:T(8,128)(2,1)}, u32[]{:S(2)}) copy-start(bf16[256,2048]{1,0:T(8,128)(2,1)} %param.11) | copy-start | bytes 3145732
Sparse Core Ops, SparseCore 0:
  9.9 56.9 all-gather.2
  68.8 54.2 all-gather.4
  153.3 171.9 all-reduce.2
  328.6 70.4 reduce-scatter.1
where the time goes:
time: 437 us
  waiting for transfers between devices  305 us (70%)
  matrix products  63.1 us (14%)
  other arithmetic  28.6 us (7%)
  blocking collectives  25.2 us (6%)
  between operations  13.9 us (3%)
    psum x1, waiting for transfers between devices, shards(): lax.psum(local_gate.astype(jnp.bfloat16), 'rep').astype(jnp.float32)  141 us
    reduce_scatter x1, waiting for transfers between devices, shards(): lax.psum_scatter((result + jnp.dot(grad_up_pre, up_weight.T, preferred_el...  66.9 us
    all_gather x1, waiting for transfers between devices, shards(): lax.all_gather(tokens_in, ('fs', 'tp'), axis=0, tiled=True)  58.2 us
    all_gather x1, waiting for transfers between devices, shards(): lax.all_gather(out_grad, ('fs', 'tp'), axis=0, tiled=True)  37.7 us
    psum x1, blocking collectives, shards(): gain_partial = lax.psum(gain_local, ('fs', 'tp'))  12.8 us
    psum x1, blocking collectives, shards(): grad_gain = lax.psum(gain_partial, 'rep')  12.4 us
    mul x1, other arithmetic, shards(): unit_rows = floats * inverse  10.4 us
    dot_general x1, matrix products, shards(): jnp.dot(hidden.T, whole_grad, preferred_element_type=jnp.float32)  10.3 us
  transfers between devices with their start and end apart: 4, of which 4 were waited for; matrix products, arithmetic and copies ran while one was open for 13% of the time, Pallas kernels for 0%

commit v1 on v0

v1 whole, which is shorter than its diff:
```python
import jax
import jax.numpy as jnp
from jax import lax
from jax.experimental import pallas as pl
from jax.experimental.pallas import tpu as pltpu
from jax.sharding import PartitionSpec as P

norm_eps = 1e-06
MESH = pl.DeviceIdType.MESH
F32, BF16 = jnp.float32, jnp.bfloat16
CHUNKS = 8
NT = (((1,), (1,)), ((), ()))


def flip(f, j):
    return (f % 2 + j % 2) % 2 + 2 * ((f // 2 + j // 2) % 2)


def remote(src, dst, send, recv, dev):
    return pltpu.make_async_remote_copy(
        src_ref=src, dst_ref=dst, send_sem=send, recv_sem=recv, device_id=dev, device_id_type=MESH
    )


def gather_kernel(
    x_ref, g_ref, gain_ref, gw_ref, uw_ref, dw_ref,
    normed_out, grad_out, hid_out, ggp_out, gup_out,
    xall, gall, normed, hid, ggp, gup, ssem, rsem, osem,
):
    f, t = lax.axis_index("fs"), lax.axis_index("tp")
    other = 1 - t
    rows = x_ref.shape[0]
    half = rows // 2
    to_a, to_b, to_p = {"fs": flip(f, 1)}, {"fs": flip(f, 2)}, {"tp": other}
    barrier = pltpu.get_barrier_semaphore()
    for dev in (to_a, to_b, to_p):
        pl.semaphore_signal(barrier, inc=1, device_id=dev, device_id_type=MESH)
    pl.semaphore_wait(barrier, 3)

    def pos(j, core):
        return flip(f, j) * 2 + core

    bufs = ((x_ref, xall), (g_ref, gall))
    low, high = pl.ds(0, half), pl.ds(half, half)

    def copy(n, kind, incoming=False):
        own, held = bufs[n]
        sems = (ssem.at[n, kind], rsem.at[n, kind])
        mine = pos(0, t)
        if kind == 0:
            return remote(own, held.at[pos(1, t) if incoming else mine], *sems, to_a)
        if kind == 1:
            return remote(own, held.at[pos(2, t) if incoming else mine], *sems, to_b)
        if kind == 2:
            return remote(own, held.at[pos(0, other) if incoming else mine], *sems, to_p)
        if kind == 3:
            slot = held.at[pos(3, t) if incoming else pos(1, t), high]
            return remote(slot, slot, *sems, to_b)
        if kind == 4:
            slot = held.at[pos(3, t) if incoming else pos(2, t), low]
            return remote(slot, slot, *sems, to_a)
        j = {5: 1, 6: 2, 7: 3, 8: 3}[kind]
        slot = held.at[pos(j, other if incoming else t)]
        if kind == 7:
            slot = slot.at[low]
        if kind == 8:
            slot = slot.at[high]
        return remote(slot, slot, *sems, to_p)

    for n in range(2):
        for kind in (0, 1, 2):
            copy(n, kind).start()
    xall[pos(0, t)] = x_ref[...]
    gall[pos(0, t)] = g_ref[...]

    def outs(p):
        return [
            pltpu.make_async_copy(src.at[p], dst.at[p], osem.at[i])
            for i, (src, dst) in enumerate(
                ((normed, normed_out), (gall, grad_out), (hid, hid_out), (ggp, ggp_out), (gup, gup_out))
            )
        ]

    def body(i, carry):
        @pl.when(i == 1)
        def _():
            for n in range(2):
                copy(n, 2, True).wait_recv()

        @pl.when(i == 2)
        def _():
            for n in range(2):
                copy(n, 0, True).wait_recv()
                copy(n, 3).start()
                copy(n, 5).start()
                copy(n, 1, True).wait_recv()
                copy(n, 4).start()
                copy(n, 6).start()

        @pl.when(i == 3)
        def _():
            for n in range(2):
                copy(n, 5, True).wait_recv()

        @pl.when(i == 5)
        def _():
            for n in range(2):
                copy(n, 6, True).wait_recv()

        @pl.when(i == 6)
        def _():
            for n in range(2):
                copy(n, 4, True).wait_recv()
                copy(n, 7).start()
                copy(n, 3, True).wait_recv()
                copy(n, 8).start()

        @pl.when(i == 7)
        def _():
            for n in range(2):
                copy(n, 7, True).wait_recv()
                copy(n, 8, True).wait_recv()

        p = flip(f, i // 2) * 2 + (t + i) % 2
        floats = xall[p].astype(F32)
        inverse = lax.rsqrt(jnp.mean(floats * floats, axis=-1, keepdims=True) + norm_eps)
        normed[p] = (floats * inverse * gain_ref[...]).astype(BF16)
        gate_pre = jnp.dot(normed[p], gw_ref[...], preferred_element_type=F32)
        up_pre = jnp.dot(normed[p], uw_ref[...], preferred_element_type=F32)
        grad_hidden = 0.5 * lax.dot_general(gall[p], dw_ref[...], NT, preferred_element_type=F32)
        sigma = jax.nn.sigmoid(gate_pre)
        active = gate_pre * sigma
        hid[p] = (active * up_pre).astype(BF16)
        ggp[p] = (grad_hidden * up_pre * sigma * (1.0 + gate_pre * (1.0 - sigma))).astype(BF16)
        gup[p] = (grad_hidden * active).astype(BF16)
        return carry

    lax.fori_loop(0, 8, body, 0)
    whole = [
        pltpu.make_async_copy(src, dst, osem.at[i])
        for i, (src, dst) in enumerate(
            ((normed, normed_out), (gall, grad_out), (hid, hid_out), (ggp, ggp_out), (gup, gup_out))
        )
    ]
    for c in whole:
        c.start()
    for n in range(2):
        for kind in range(9):
            copy(n, kind).wait_send()
    for c in whole:
        c.wait()


def exit_kernel(
    reps,
    ggp_ref, gup_ref, gw_ref, uw_ref, wd_ref, wg_ref, wu_ref,
    gn_ref, fd_ref, fg_ref, fu_ref,
    ind, ing, inu, tbuf, pin, sbuf, rsin,
    up_send, in_recv, fin_recv, down_send, p_send, p_recv, s_send, s_recv,
):
    f, t, r = lax.axis_index("fs"), lax.axis_index("tp"), lax.axis_index("rep")
    other = 1 - t
    middle = reps // 2
    sign = 1 - 2 * (r // middle)
    up, down = {"rep": r + sign}, {"rep": (r - sign + reps) % reps}
    right = r // middle
    depth = (1 - right) * (middle - 1 - r) + right * (r - middle)
    center, outer = depth == 0, depth == middle - 1
    inner, has_down = depth > 0, depth < middle - 1
    peers = [{"fs": flip(f, 1)}, {"fs": flip(f, 2)}, {"fs": flip(f, 3)}, {"tp": other}, up]
    barrier = pltpu.get_barrier_semaphore()
    for dev in peers:
        pl.semaphore_signal(barrier, inc=1, device_id=dev, device_id_type=MESH)

    @pl.when(has_down)
    def _():
        pl.semaphore_signal(barrier, inc=1, device_id=down, device_id_type=MESH)
        pl.semaphore_wait(barrier, 6)

    @pl.when(outer)
    def _():
        pl.semaphore_wait(barrier, 5)

    arrays = ((wd_ref, ind, fd_ref), (wg_ref, ing, fg_ref), (wu_ref, inu, fu_ref))
    rows = gn_ref.shape[0]
    width = gw_ref.shape[0]
    tile = min(512, width)

    def at(ref, s):
        step = ref.shape[0] // CHUNKS
        return ref.at[pl.ds(pl.multiple_of(s * step, step), step)]

    def up_copy(a, s, src, dst, recv):
        return remote(at(src, s), at(dst, s), up_send.at[a, s], recv.at[a, s], up)

    def down_copy(a, s):
        fin = arrays[a][2]
        return remote(at(fin, s), at(fin, s), down_send.at[a, s], fin_recv.at[a, s], down)

    @pl.when(outer)
    def _():
        def first(s, carry):
            for a, (own, inc, fin) in enumerate(arrays):
                up_copy(a, s, own, inc, in_recv).start()
            return carry

        lax.fori_loop(0, CHUNKS, first, 0)

    def pair_copy(j):
        return remote(tbuf.at[j], pin.at[j], p_send.at[j], p_recv.at[j], {"tp": other})

    def peer_copy(j):
        return remote(sbuf.at[j], rsin.at[j], s_send.at[j], s_recv.at[j], {"fs": flip(f, j)})

    def term(owner, c):
        here = pl.ds(pl.multiple_of(owner * rows, rows), rows)
        cols = pl.ds(pl.multiple_of(c * tile, tile), tile)
        out = lax.dot_general(ggp_ref[here, :], gw_ref[cols, :], NT, preferred_element_type=F32)
        out = out + lax.dot_general(gup_ref[here, :], uw_ref[cols, :], NT, preferred_element_type=F32)
        return out.astype(BF16), cols

    def body(s, carry):
        j = 3 - s % 4

        @pl.when(s < 4)
        def _():
            def one(c, carry):
                value, cols = term(flip(f, j) * 2 + other, c)
                tbuf[j, :, cols] = value
                return carry

            lax.fori_loop(0, width // tile, one, 0)
            pair_copy(j).start()

        @pl.when((s >= 4) & (s < 8))
        def _():
            pair_copy(j).wait_recv()

            def one(c, carry):
                value, cols = term(flip(f, j) * 2 + t, c)
                total = value.astype(F32) + pin[j, :, cols].astype(F32)
                gn_ref[:, cols] = total
                sbuf[j, :, cols] = total.astype(BF16)
                return carry

            lax.fori_loop(0, width // tile, one, 0)

            @pl.when(j > 0)
            def _():
                peer_copy(j).start()

        @pl.when((s < CHUNKS) & has_down)
        def _():
            for a, (own, inc, fin) in enumerate(arrays):
                up_copy(a, s, inc, inc, in_recv).wait_recv()
                here = at(inc, s)
                here[...] = (at(own, s)[...].astype(F32) + here[...].astype(F32)).astype(BF16)

                @pl.when(center)
                def _():
                    up_copy(a, s, inc, fin, fin_recv).start()

                @pl.when(inner)
                def _():
                    up_copy(a, s, inc, inc, in_recv).start()

        @pl.when(s >= 1)
        def _():
            for a, (own, inc, fin) in enumerate(arrays):
                before = s - 1
                down_copy(a, before).wait_recv()

                @pl.when(center)
                def _():
                    here = at(fin, before)
                    here[...] = (at(inc, before)[...].astype(F32) + here[...].astype(F32)).astype(BF16)

                @pl.when(has_down)
                def _():
                    down_copy(a, before).start()

        return carry

    lax.fori_loop(0, CHUNKS + 1, body, 0)
    for j in (3, 2, 1):
        peer_copy(j).wait_recv()
    gn_ref[...] = gn_ref[...] + rsin[3].astype(F32) + rsin[2].astype(F32) + rsin[1].astype(F32)
    for j in (3, 2, 1):
        peer_copy(j).wait_send()
    for j in range(4):
        pair_copy(j).wait_send()

    def last(s, carry):
        for a, (own, inc, fin) in enumerate(arrays):
            up_copy(a, s, own, inc, in_recv).wait_send()

            @pl.when(has_down)
            def _():
                down_copy(a, s).wait_send()

        return carry

    lax.fori_loop(0, CHUNKS, last, 0)


def shards(tokens_in, norm_gain, gate_weight, up_weight, down_weight, out_grad):
    rows, d = tokens_in.shape
    ff = gate_weight.shape[1]
    reps = lax.axis_size("rep")
    ranks = lax.axis_size("fs") * lax.axis_size("tp")
    factor = float(rows * reps * ranks) ** (-0.5)
    vmem, anywhere = pl.BlockSpec(memory_space=pltpu.VMEM), pl.BlockSpec(memory_space=pl.ANY)
    wide, narrow = (ranks, rows, d), (ranks, rows, ff)
    dma = pltpu.SemaphoreType.DMA
    flat = (ranks * rows,)
    gathered = pl.pallas_call(
        gather_kernel,
        out_shape=[jax.ShapeDtypeStruct(s, BF16) for s in (wide, wide, narrow, narrow, narrow)],
        in_specs=[vmem] * 6,
        out_specs=[anywhere] * 5,
        scratch_shapes=[
            pltpu.VMEM(wide, BF16), pltpu.VMEM(wide, BF16), pltpu.VMEM(wide, BF16),
            pltpu.VMEM(narrow, BF16), pltpu.VMEM(narrow, BF16), pltpu.VMEM(narrow, BF16),
            dma((2, 9)), dma((2, 9)), dma((5,)),
        ],
        compiler_params=pltpu.CompilerParams(
            collective_id=0, has_side_effects=True, vmem_limit_bytes=60 * 2**20
        ),
        name="gather_forward",
    )(tokens_in, out_grad, norm_gain.reshape(1, d), gate_weight, up_weight, down_weight)
    normed, whole_grad, hidden, ggp, gup = [a.reshape(flat + a.shape[2:]) for a in gathered]
    local_down = jnp.dot(hidden.T, whole_grad, preferred_element_type=F32).astype(BF16)
    local_gate = jnp.dot(normed.T, ggp, preferred_element_type=F32).astype(BF16)
    local_up = jnp.dot(normed.T, gup, preferred_element_type=F32).astype(BF16)
    tall, long = (d, ff), (ff, d)
    block4 = (4, rows, d)
    grad_normed, sum_down, sum_gate, sum_up = pl.pallas_call(
        lambda *refs: exit_kernel(reps, *refs),
        out_shape=[
            jax.ShapeDtypeStruct((rows, d), F32),
            jax.ShapeDtypeStruct(long, BF16),
            jax.ShapeDtypeStruct(tall, BF16),
            jax.ShapeDtypeStruct(tall, BF16),
        ],
        in_specs=[vmem] * 7,
        out_specs=[vmem] * 4,
        scratch_shapes=[
            pltpu.VMEM(long, BF16), pltpu.VMEM(tall, BF16), pltpu.VMEM(tall, BF16),
            pltpu.VMEM(block4, BF16), pltpu.VMEM(block4, BF16), pltpu.VMEM(block4, BF16), pltpu.VMEM(block4, BF16),
            dma((3, CHUNKS)), dma((3, CHUNKS)), dma((3, CHUNKS)), dma((3, CHUNKS)),
            dma((4,)), dma((4,)), dma((4,)), dma((4,)),
        ],
        compiler_params=pltpu.CompilerParams(
            collective_id=1, has_side_effects=True, vmem_limit_bytes=60 * 2**20
        ),
        name="reduce_exit",
    )(ggp, gup, gate_weight, up_weight, local_down, local_gate, local_up)
    grad_gate = sum_gate.astype(F32) * factor
    grad_up = sum_up.astype(F32) * factor
    grad_down = sum_down.astype(F32) * (0.5 * factor)
    floats = tokens_in.astype(F32)
    inverse = lax.rsqrt(jnp.mean(floats * floats, axis=-1, keepdims=True) + norm_eps)
    unit = floats * inverse
    grad_gain = lax.psum(jnp.sum(grad_normed * unit, axis=0), ("rep", "fs", "tp"))
    scaled = grad_normed * norm_gain
    grad_in = (
        out_grad.astype(F32)
        + inverse * scaled
        - unit * inverse * jnp.mean(scaled * unit, axis=-1, keepdims=True)
    )
    return (grad_in.astype(BF16), grad_gain, grad_gate, grad_up, grad_down)


def solution(mesh):
    spread = ("fs", "tp")
    in_specs = (
        P(("rep", "fs", "tp"), None), P(), P(None, spread), P(None, spread), P(spread, None),
        P(("rep", "fs", "tp"), None),
    )
    out_specs = (
        P(("rep", "fs", "tp"), None), P(), P(None, spread), P(None, spread), P(spread, None),
    )
    return jax.shard_map(shards, mesh=mesh, in_specs=in_specs, out_specs=out_specs, check_vma=False)
```

time: 437 us -> 297 us (0.68)
  waiting for transfers between devices: 305 us -> 0 us
  Pallas kernels: 0 us -> 226 us
  matrix products: 63.1 us -> 19.9 us
  other arithmetic: 28.6 us -> 11.3 us
  blocking collectives: 25.2 us -> 38.8 us
  between operations: 13.9 us -> 0.73 us
    pallas_call x0 -> x2, Pallas kernels: none -> 226 us  [the longest x1 140 us: shards(): pl.pallas_call(lambda *refs: exit_kernel(reps, *refs), out_shape=[jax.Sha...]
    psum x1 -> x0, waiting for transfers between devices: 141 us -> none  [shards(): lax.psum(local_gate.astype(jnp.bfloat16), 'rep').astype(jnp.float32)]
    all_gather x2 -> x0, waiting for transfers between devices: 95.9 us -> none  [the longest x1 58.2 us: shards(): lax.all_gather(tokens_in, ('fs', 'tp'), axis=0, tiled=True)]
    reduce_scatter x1 -> x0, waiting for transfers between devices: 66.9 us -> none  [shards(): lax.psum_scatter((result + jnp.dot(grad_up_pre, up_weight.T, preferred_el...]
    dot_general x8 -> x3, matrix products: 63.1 us -> 19.9 us  [the longest x1 8.62 us: shards(): jnp.dot(hidden.T, whole_grad, preferred_element_type=F32).astype(BF16)]
    psum x2 -> x1, blocking collectives: 25.2 us -> 38.8 us  [shards(): lax.psum(jnp.sum(grad_normed * unit, axis=0), ('rep', 'fs', 'tp'))]
    mul x3 -> x2, other arithmetic: 17.2 us -> 6.84 us  [the longest x1 4.78 us: shards(): grad_up = sum_up.astype(F32) * factor]
    reduce_sum x1, other arithmetic: 5.23 us -> 0.29 us  [shards(): jnp.mean(floats * floats, axis=-1, keepdims=True) + norm_eps]
  transfers between devices with their start and end apart: 4 -> 0, of which waited for: 4 -> 0; matrix products, arithmetic and copies ran while one was open for 13% -> 0% of each run, Pallas kernels for 0% -> 0%
where the time goes in v1:
time: 297 us; the launch traced here: 296 us
  Pallas kernels  226 us (76%)
  blocking collectives  38.8 us (13%)
  matrix products  19.9 us (7%)
  other arithmetic  11.3 us (4%)
    pallas_call x1, Pallas kernels, shards(): pl.pallas_call(lambda *refs: exit_kernel(reps, *refs), out_shape=[jax.Sha...  140 us
    pallas_call x1, Pallas kernels, shards(): pl.pallas_call(gather_kernel, out_shape=[jax.ShapeDtypeStruct(s, BF16) fo...  85.5 us
    psum x1, blocking collectives, shards(): lax.psum(jnp.sum(grad_normed * unit, axis=0), ('rep', 'fs', 'tp'))  38.8 us
    dot_general x1, matrix products, shards(): jnp.dot(hidden.T, whole_grad, preferred_element_type=F32).astype(BF16)  8.62 us

profile of v1, /device:TPU:0, one launch (start us, length us, event | category | flops | bytes accessed | tf_op | source)
XLA Modules:
  0.0 296.5 jit_solution(9877854991352534400)
XLA Ops:
  0.6 85.5 %gather_forward.1 = (bf16[8,256,2048]{2,1,0:T(8,128)(2,1)}, bf16[8,256,2048]{2,1,0:T(8,128)(2,1)}, bf16[8,256,384]{2,1,0:T(8,128)(2,1)}, bf16[8,256,384]{2,1,0:T(8,128)(2,1)}, bf16[8,256,384]{2,1,0:T(8,128)(2,1)}) custom-call(bf16[256,2048]{1,0:T(8,128)(2,1)} %x_ref.1, bf16[256,2048]{1,0:T(8,128)(2,1)} %g_ref.1, f32[1,2048]{1,0:T(1,128)} %bitcast.17, ...), custom_call_target="tpu_custom_call" | custom-call | tf_op jit(solution)/shard_map/gather_forward/pallas_call | solution.py:316
  86.2 0.0 copy-start.5
  86.2 0.0 copy-start.8
  86.2 8.6 %bitcast_convert_fusion.2.refs_4_ = bf16[384,2048]{1,0:T(8,128)(2,1)} fusion(bf16[8,256,384]{2,1,0:T(8,128)(2,1)} %get-tuple-element.16, bf16[8,256,2048]{2,1,0:T(8,128)(2,1)} %get-tuple-element.17), kind=kOutput, calls=%fused_computation.2 | convolution fusion | flops 3222011904 | bytes 11534336 | tf_op jit(solution)/shard_map/dot_general | solution.py:332
  94.8 0.0 copy-done.5
  94.8 0.0 copy-done.8
  94.8 0.0 copy-start.6
  94.8 5.6 %bitcast_convert_fusion.1.refs_5_ = bf16[2048,384]{1,0:T(8,128)(2,1)} fusion(bf16[8,256,2048]{2,1,0:T(8,128)(2,1)S(1)} %copy-done.8, bf16[8,256,384]{2,1,0:T(8,128)(2,1)S(1)} %copy-done.5), kind=kOutput, calls=%fused_computation.1 | convolution fusion | flops 3222011904 | bytes 11534336 | tf_op jit(solution)/shard_map/dot_general | solution.py:333
  100.5 0.0 copy-done.6
  100.5 5.6 %bitcast_convert_fusion.refs_6_ = bf16[2048,384]{1,0:T(8,128)(2,1)} fusion(bf16[8,256,2048]{2,1,0:T(8,128)(2,1)S(1)} %copy-done.8, bf16[8,256,384]{2,1,0:T(8,128)(2,1)S(1)} %copy-done.6), kind=kOutput, calls=%fused_computation | convolution fusion | flops 3222011904 | bytes 11534336 | tf_op jit(solution)/shard_map/dot_general | solution.py:334
  106.1 0.0 copy-start
  106.1 0.0 copy-start.7
  106.1 140.2 %reduce_exit.1 = (f32[256,2048]{1,0:T(8,128)}, bf16[384,2048]{1,0:T(8,128)(2,1)}, bf16[2048,384]{1,0:T(8,128)(2,1)}, bf16[2048,384]{1,0:T(8,128)(2,1)}) custom-call(bf16[2048,384]{1,0:T(8,128)(2,1)} %bitcast.15, bf16[2048,384]{1,0:T(8,128)(2,1)} %bitcast.16, bf16[2048,384]{1,0:T(8,128)(2,1)} %refs_2_.1, bf16[2048,384]{1,0:T(8,128)(2,1)} %refs_3_.1, ...), custom_call_target="tpu_custom_call" | custom-call | tf_op jit(solution)/shard_map/reduce_exit/pallas_call | solution.py:337
  246.3 0.0 copy-done
  246.3 0.0 copy-start.1
  246.3 0.0 copy-start.2
  246.3 0.3 fusion.8
  246.6 0.0 copy-done.7
  246.6 2.4 fusion.7
  249.1 0.0 copy-done.1
  249.1 0.0 copy-done.2
  249.1 0.0 copy-start.3
  249.1 1.8 fusion.5
  250.9 38.8 %psum.7 = f32[2048]{0:T(1024)} all-reduce(f32[2048]{0:T(1024)S(1)} %get-tuple-element.23), channel_id=1, replica_groups=mesh['rep'=4,'fs'=4,'tp'=2] {'rep','fs','tp'}, use_global_device_ids=true, to_apply=%region_3.0 | all-reduce | flops 2048 | bytes 16384 | tf_op jit(solution)/shard_map/psum | solution.py:364
  289.6 0.0 copy-done.3
  289.6 0.0 copy-start.4
  289.6 4.8 %convert_multiply_fusion.1 = (f32[2048,384]{1,0:T(8,128)}, f32[2048,384]{1,0:T(8,128)}) fusion(bf16[2048,384]{1,0:T(8,128)(2,1)} %get-tuple-element.21, bf16[2048,384]{1,0:T(8,128)(2,1)S(1)} %copy-done.3), kind=kLoop, calls=%fused_computation.4 | loop fusion | flops 3145728 | bytes 9437184 | tf_op jit(solution)/shard_map/mul | solution.py:359
  294.4 0.0 copy-done.4
  294.4 2.1 convert_multiply_fusion
  (2 shorter events, 0.0 us)
Async XLA Ops:
  86.2 8.6 %copy-start.5 = (bf16[8,256,384]{2,1,0:T(8,128)(2,1)S(1)}, bf16[8,256,384]{2,1,0:T(8,128)(2,1)}, u32[]{:S(2)}) copy-start(bf16[8,256,384]{2,1,0:T(8,128)(2,1)} %get-tuple-element.14) | copy-start | bytes 4718596
  86.2 8.6 %copy-start.8 = (bf16[8,256,2048]{2,1,0:T(8,128)(2,1)S(1)}, bf16[8,256,2048]{2,1,0:T(8,128)(2,1)}, u32[]{:S(2)}) copy-start(bf16[8,256,2048]{2,1,0:T(8,128)(2,1)} %get-tuple-element.18) | copy-start | bytes 25165828
  94.8 5.6 %copy-start.6 = (bf16[8,256,384]{2,1,0:T(8,128)(2,1)S(1)}, bf16[8,256,384]{2,1,0:T(8,128)(2,1)}, u32[]{:S(2)}) copy-start(bf16[8,256,384]{2,1,0:T(8,128)(2,1)} %get-tuple-element.15) | copy-start | bytes 4718596
  106.1 140.2 %copy-start = (bf16[256,2048]{1,0:T(8,128)(2,1)S(1)}, bf16[256,2048]{1,0:T(8,128)(2,1)}, u32[]{:S(2)}) copy-start(bf16[256,2048]{1,0:T(8,128)(2,1)} %x_ref.1) | copy-start | bytes 3145732
  106.1 140.5 %copy-start.7 = (f32[2048]{0:T(1024)S(1)}, f32[2048]{0:T(1024)}, u32[]{:S(2)}) copy-start(f32[2048]{0:T(1024)} %param.7) | copy-start | bytes 24580
  246.3 2.7 copy-start.1
  246.3 2.7 copy-start.2
  249.1 40.6 %copy-start.3 = (bf16[2048,384]{1,0:T(8,128)(2,1)S(1)}, bf16[2048,384]{1,0:T(8,128)(2,1)}, u32[]{:S(2)}) copy-start(bf16[2048,384]{1,0:T(8,128)(2,1)} %get-tuple-element.20) | copy-start | bytes 4718596
  289.6 4.8 %copy-start.4 = (bf16[384,2048]{1,0:T(8,128)(2,1)S(1)}, bf16[384,2048]{1,0:T(8,128)(2,1)}, u32[]{:S(2)}) copy-start(bf16[384,2048]{1,0:T(8,128)(2,1)} %get-tuple-element.22) | copy-start | bytes 4718596

commit v2 on v1

--- a/solution.py
+++ b/solution.py
@@ -73,14 +73,6 @@
     xall[pos(0, t)] = x_ref[...]
     gall[pos(0, t)] = g_ref[...]
 
-    def outs(p):
-        return [
-            pltpu.make_async_copy(src.at[p], dst.at[p], osem.at[i])
-            for i, (src, dst) in enumerate(
-                ((normed, normed_out), (gall, grad_out), (hid, hid_out), (ggp, ggp_out), (gup, gup_out))
-            )
-        ]
-
     def body(i, carry):
         @pl.when(i == 1)
         def _():
@@ -153,10 +145,11 @@
 
 def exit_kernel(
     reps,
-    ggp_ref, gup_ref, gw_ref, uw_ref, wd_ref, wg_ref, wu_ref,
-    gn_ref, fd_ref, fg_ref, fu_ref,
-    ind, ing, inu, tbuf, pin, sbuf, rsin,
+    x_ref, ggp_ref, gup_ref, gw_ref, uw_ref, wd_ref, wg_ref, wu_ref,
+    gn_ref, gain_ref, fd_ref, fg_ref, fu_ref,
+    ind, ing, inu, tbuf, pin, sbuf, rsin, gbuf, rbuf,
     up_send, in_recv, fin_recv, down_send, p_send, p_recv, s_send, s_recv,
+    g_send, g_recv, r_send, r_recv,
 ):
     f, t, r = lax.axis_index("fs"), lax.axis_index("tp"), lax.axis_index("rep")
     other = 1 - t
@@ -167,19 +160,17 @@
     depth = (1 - right) * (middle - 1 - r) + right * (r - middle)
     center, outer = depth == 0, depth == middle - 1
     inner, has_down = depth > 0, depth < middle - 1
-    peers = [{"fs": flip(f, 1)}, {"fs": flip(f, 2)}, {"fs": flip(f, 3)}, {"tp": other}, up]
+    group = []
+    for j in range(4):
+        for k in range(2):
+            if j or k:
+                core = (t + k) % 2
+                group.append((flip(f, j) * 2 + core, {"fs": flip(f, j), "tp": core}))
+    far = [((r + k) % reps, (r - k + reps) % reps) for k in range(1, reps)]
     barrier = pltpu.get_barrier_semaphore()
-    for dev in peers:
+    for dev in [dev for _, dev in group] + [{"rep": to} for to, _ in far]:
         pl.semaphore_signal(barrier, inc=1, device_id=dev, device_id_type=MESH)
-
-    @pl.when(has_down)
-    def _():
-        pl.semaphore_signal(barrier, inc=1, device_id=down, device_id_type=MESH)
-        pl.semaphore_wait(barrier, 6)
-
-    @pl.when(outer)
-    def _():
-        pl.semaphore_wait(barrier, 5)
+    pl.semaphore_wait(barrier, len(group) + len(far))
 
     arrays = ((wd_ref, ind, fd_ref), (wg_ref, ing, fg_ref), (wu_ref, inu, fu_ref))
     rows = gn_ref.shape[0]
@@ -219,20 +210,66 @@
         out = out + lax.dot_general(gup_ref[here, :], uw_ref[cols, :], NT, preferred_element_type=F32)
         return out.astype(BF16), cols
 
+    mine = f * 2 + t
+
+    def group_copy(n, incoming=False):
+        where, dev = group[n]
+        slot = gbuf.at[where if incoming else mine]
+        return remote(gbuf.at[mine], slot, g_send.at[n], g_recv.at[n], dev)
+
+    def far_copy(n, incoming=False):
+        to, source = far[n]
+        slot = rbuf.at[source if incoming else r]
+        return remote(rbuf.at[r], slot, r_send.at[n], r_recv.at[n], {"rep": to})
+
+    def for_partner(i, carry):
+        j = 3 - i
+
+        def one(c, carry):
+            value, cols = term(flip(f, j) * 2 + other, c)
+            tbuf[j, :, cols] = value
+            return carry
+
+        lax.fori_loop(0, width // tile, one, 0)
+        pair_copy(j).start()
+        return carry
+
+    lax.fori_loop(0, 4, for_partner, 0)
+
+    def inward(a, s):
+        own, inc, fin = arrays[a]
+
+        @pl.when(has_down)
+        def _():
+            up_copy(a, s, inc, inc, in_recv).wait_recv()
+            here = at(inc, s)
+            here[...] = (at(own, s)[...].astype(F32) + here[...].astype(F32)).astype(BF16)
+
+            @pl.when(center)
+            def _():
+                up_copy(a, s, inc, fin, fin_recv).start()
+
+            @pl.when(inner)
+            def _():
+                up_copy(a, s, inc, inc, in_recv).start()
+
+    def outward(a, s):
+        own, inc, fin = arrays[a]
+        down_copy(a, s).wait_recv()
+
+        @pl.when(center)
+        def _():
+            here = at(fin, s)
+            here[...] = (at(inc, s)[...].astype(F32) + here[...].astype(F32)).astype(BF16)
+
+        @pl.when(has_down)
+        def _():
+            down_copy(a, s).start()
+
     def body(s, carry):
         j = 3 - s % 4
 
         @pl.when(s < 4)
-        def _():
-            def one(c, carry):
-                value, cols = term(flip(f, j) * 2 + other, c)
-                tbuf[j, :, cols] = value
-                return carry
-
-            lax.fori_loop(0, width // tile, one, 0)
-            pair_copy(j).start()
-
-        @pl.when((s >= 4) & (s < 8))
         def _():
             pair_copy(j).wait_recv()
 
@@ -249,42 +286,59 @@
             def _():
                 peer_copy(j).start()
 
-        @pl.when((s < CHUNKS) & has_down)
-        def _():
-            for a, (own, inc, fin) in enumerate(arrays):
-                up_copy(a, s, inc, inc, in_recv).wait_recv()
-                here = at(inc, s)
-                here[...] = (at(own, s)[...].astype(F32) + here[...].astype(F32)).astype(BF16)
-
-                @pl.when(center)
+        for a in range(3):
+
+            @pl.when(s < CHUNKS)
+            def _():
+                inward(a, s)
+
+            if a < 2:
+
+                @pl.when(s >= 1)
                 def _():
-                    up_copy(a, s, inc, fin, fin_recv).start()
-
-                @pl.when(inner)
+                    outward(a + 1, s - 1)
+
+            else:
+
+                @pl.when(s < CHUNKS)
                 def _():
-                    up_copy(a, s, inc, inc, in_recv).start()
-
-        @pl.when(s >= 1)
-        def _():
-            for a, (own, inc, fin) in enumerate(arrays):
-                before = s - 1
-                down_copy(a, before).wait_recv()
-
-                @pl.when(center)
-                def _():
-                    here = at(fin, before)
-                    here[...] = (at(inc, before)[...].astype(F32) + here[...].astype(F32)).astype(BF16)
-
-                @pl.when(has_down)
-                def _():
-                    down_copy(a, before).start()
+                    outward(0, s)
+
+        @pl.when(s == CHUNKS - 1)
+        def _():
+            for k in (3, 2, 1):
+                peer_copy(k).wait_recv()
+
+            def one(c, carry):
+                cols = pl.ds(pl.multiple_of(c * tile, tile), tile)
+                total = gn_ref[:, cols]
+                for k in (3, 2, 1):
+                    total = total + rsin[k, :, cols].astype(F32)
+                gn_ref[:, cols] = total
+                return carry
+
+            lax.fori_loop(0, width // tile, one, 0)
+            floats = x_ref[...].astype(F32)
+            inverse = lax.rsqrt(jnp.mean(floats * floats, axis=-1, keepdims=True) + norm_eps)
+            gbuf[mine] = jnp.sum(gn_ref[...] * (floats * inverse), axis=0, keepdims=True)
+            for n in range(len(group)):
+                group_copy(n).start()
 
         return carry
 
     lax.fori_loop(0, CHUNKS + 1, body, 0)
-    for j in (3, 2, 1):
-        peer_copy(j).wait_recv()
-    gn_ref[...] = gn_ref[...] + rsin[3].astype(F32) + rsin[2].astype(F32) + rsin[1].astype(F32)
+    for n in range(len(group)):
+        group_copy(n, True).wait_recv()
+    rbuf[r] = jnp.sum(gbuf[...], axis=0)
+    for n in range(len(far)):
+        far_copy(n).start()
+    for n in range(len(far)):
+        far_copy(n, True).wait_recv()
+    gain_ref[...] = jnp.sum(rbuf[...], axis=0)
+    for n in range(len(group)):
+        group_copy(n).wait_send()
+    for n in range(len(far)):
+        far_copy(n).wait_send()
     for j in (3, 2, 1):
         peer_copy(j).wait_send()
     for j in range(4):
@@ -334,41 +388,43 @@
     local_up = jnp.dot(normed.T, gup, preferred_element_type=F32).astype(BF16)
     tall, long = (d, ff), (ff, d)
     block4 = (4, rows, d)
-    grad_normed, sum_down, sum_gate, sum_up = pl.pallas_call(
+    grad_normed, grad_gain, sum_down, sum_gate, sum_up = pl.pallas_call(
         lambda *refs: exit_kernel(reps, *refs),
         out_shape=[
             jax.ShapeDtypeStruct((rows, d), F32),
+            jax.ShapeDtypeStruct((1, d), F32),
             jax.ShapeDtypeStruct(long, BF16),
             jax.ShapeDtypeStruct(tall, BF16),
             jax.ShapeDtypeStruct(tall, BF16),
         ],
-        in_specs=[vmem] * 7,
-        out_specs=[vmem] * 4,
+        in_specs=[vmem] * 8,
+        out_specs=[vmem] * 5,
         scratch_shapes=[
             pltpu.VMEM(long, BF16), pltpu.VMEM(tall, BF16), pltpu.VMEM(tall, BF16),
             pltpu.VMEM(block4, BF16), pltpu.VMEM(block4, BF16), pltpu.VMEM(block4, BF16), pltpu.VMEM(block4, BF16),
+            pltpu.VMEM((ranks, 1, d), F32), pltpu.VMEM((reps, 1, d), F32),
             dma((3, CHUNKS)), dma((3, CHUNKS)), dma((3, CHUNKS)), dma((3, CHUNKS)),
             dma((4,)), dma((4,)), dma((4,)), dma((4,)),
+            dma((ranks,)), dma((ranks,)), dma((reps,)), dma((reps,)),
         ],
         compiler_params=pltpu.CompilerParams(
             collective_id=1, has_side_effects=True, vmem_limit_bytes=60 * 2**20
         ),
         name="reduce_exit",
-    )(ggp, gup, gate_weight, up_weight, local_down, local_gate, local_up)
+    )(tokens_in, ggp, gup, gate_weight, up_weight, local_down, local_gate, local_up)
     grad_gate = sum_gate.astype(F32) * factor
     grad_up = sum_up.astype(F32) * factor
     grad_down = sum_down.astype(F32) * (0.5 * factor)
     floats = tokens_in.astype(F32)
     inverse = lax.rsqrt(jnp.mean(floats * floats, axis=-1, keepdims=True) + norm_eps)
     unit = floats * inverse
-    grad_gain = lax.psum(jnp.sum(grad_normed * unit, axis=0), ("rep", "fs", "tp"))
     scaled = grad_normed * norm_gain
     grad_in = (
         out_grad.astype(F32)
         + inverse * scaled
         - unit * inverse * jnp.mean(scaled * unit, axis=-1, keepdims=True)
     )
-    return (grad_in.astype(BF16), grad_gain, grad_gate, grad_up, grad_down)
+    return (grad_in.astype(BF16), grad_gain.reshape(d), grad_gate, grad_up, grad_down)
 
 
 def solution(mesh):

time: 297 us -> 251 us (0.85)
  blocking collectives: 38.8 us -> 0 us
  Pallas kernels: 226 us -> 220 us
    psum x1 -> x0, blocking collectives: 38.8 us -> none  [shards(): lax.psum(jnp.sum(grad_normed * unit, axis=0), ('rep', 'fs', 'tp'))]
    pallas_call x1, Pallas kernels: 140 us -> 134 us  [shards(): pl.pallas_call(lambda *refs: exit_kernel(reps, *refs), out_shape=[jax.Sha...]
where the time goes in v2:
time: 251 us
  Pallas kernels  220 us (88%)
  matrix products  19.9 us (8%)
  other arithmetic  9.63 us (4%)
    pallas_call x1, Pallas kernels, shards(): pl.pallas_call(lambda *refs: exit_kernel(reps, *refs), out_shape=[jax.Sha...  134 us
    pallas_call x1, Pallas kernels, shards(): pl.pallas_call(gather_kernel, out_shape=[jax.ShapeDtypeStruct(s, BF16) fo...  85.5 us
    dot_general x1, matrix products, shards(): jnp.dot(hidden.T, whole_grad, preferred_element_type=F32).astype(BF16)  8.62 us
    dot_general x1, matrix products, shards(): local_gate = jnp.dot(normed.T, ggp, preferred_element_type=F32).astype(BF16)  5.64 us
    dot_general x1, matrix products, shards(): local_up = jnp.dot(normed.T, gup, preferred_element_type=F32).astype(BF16)  5.63 us

profile of v2, /device:TPU:0, one launch (start us, length us, event | category | flops | bytes accessed | tf_op | source)
XLA Modules:
  0.0 250.9 jit_solution(2619049182503729740)
XLA Ops:
  0.6 85.5 %gather_forward.1 = (bf16[8,256,2048]{2,1,0:T(8,128)(2,1)}, bf16[8,256,2048]{2,1,0:T(8,128)(2,1)}, bf16[8,256,384]{2,1,0:T(8,128)(2,1)}, bf16[8,256,384]{2,1,0:T(8,128)(2,1)}, bf16[8,256,384]{2,1,0:T(8,128)(2,1)}) custom-call(bf16[256,2048]{1,0:T(8,128)(2,1)} %refs_0_.1, bf16[256,2048]{1,0:T(8,128)(2,1)} %g_ref.1, f32[1,2048]{1,0:T(1,128)} %bitcast.18, ...), custom_call_target="tpu_custom_call" | custom-call | tf_op jit(solution)/shard_map/gather_forward/pallas_call | solution.py:370
  86.2 0.0 copy-start.6
  86.2 0.0 copy-start.10
  86.2 8.6 %bitcast_convert_fusion.2.refs_5_ = bf16[384,2048]{1,0:T(8,128)(2,1)} fusion(bf16[8,256,384]{2,1,0:T(8,128)(2,1)} %get-tuple-element.17, bf16[8,256,2048]{2,1,0:T(8,128)(2,1)} %get-tuple-element.18), kind=kOutput, calls=%fused_computation.2 | convolution fusion | flops 3222011904 | bytes 11534336 | tf_op jit(solution)/shard_map/dot_general | solution.py:386
  94.8 0.0 copy-done.6
  94.8 0.0 copy-done.10
  94.8 0.0 copy-start.7
  94.8 5.6 %bitcast_convert_fusion.1.refs_6_ = bf16[2048,384]{1,0:T(8,128)(2,1)} fusion(bf16[8,256,2048]{2,1,0:T(8,128)(2,1)S(1)} %copy-done.10, bf16[8,256,384]{2,1,0:T(8,128)(2,1)S(1)} %copy-done.6), kind=kOutput, calls=%fused_computation.1 | convolution fusion | flops 3222011904 | bytes 11534336 | tf_op jit(solution)/shard_map/dot_general | solution.py:387
  100.5 0.0 copy-done.7
  100.5 5.6 %bitcast_convert_fusion.refs_7_ = bf16[2048,384]{1,0:T(8,128)(2,1)} fusion(bf16[8,256,2048]{2,1,0:T(8,128)(2,1)S(1)} %copy-done.10, bf16[8,256,384]{2,1,0:T(8,128)(2,1)S(1)} %copy-done.7), kind=kOutput, calls=%fused_computation | convolution fusion | flops 3222011904 | bytes 11534336 | tf_op jit(solution)/shard_map/dot_general | solution.py:388
  106.1 0.0 copy-start
  106.1 0.0 copy-start.8
  106.1 134.1 %reduce_exit.1 = (f32[256,2048]{1,0:T(8,128)}, f32[1,2048]{1,0:T(1,128)}, bf16[384,2048]{1,0:T(8,128)(2,1)}, bf16[2048,384]{1,0:T(8,128)(2,1)}, bf16[2048,384]{1,0:T(8,128)(2,1)}) custom-call(bf16[256,2048]{1,0:T(8,128)(2,1)} %refs_0_.1, bf16[2048,384]{1,0:T(8,128)(2,1)} %bitcast.16, bf16[2048,384]{1,0:T(8,128)(2,1)} %bitcast.17, bf16[2048,384]{1,0:T(8,128)(2,1)} %refs_3_.1, ...), custom_call_target="tpu_custom_call" | custom-call | tf_op jit(solution)/shard_map/reduce_exit/pallas_call | solution.py:391
  240.2 0.0 copy-done
  240.2 0.0 copy-start.1
  240.3 0.0 copy-start.2
  240.3 0.3 fusion.6
  240.6 0.0 copy-done.8
  240.6 2.2 fusion.5
  242.8 0.0 copy-done.1
  242.8 0.0 copy-done.2
  242.8 0.0 copy-start.3
  242.8 0.0 copy-start.4
  242.9 1.8 fusion.4
  244.6 0.0 copy-done.3
  244.6 0.3 copy-done.4
  245.0 0.0 copy-start.5
  245.0 3.3 %convert_multiply_fusion.1 = (f32[2048,384]{1,0:T(8,128)}, f32[2048,384]{1,0:T(8,128)}) fusion(bf16[2048,384]{1,0:T(8,128)(2,1)S(1)} %copy-done.4, bf16[2048,384]{1,0:T(8,128)(2,1)S(1)} %copy-done.3), kind=kLoop, calls=%fused_computation.4 | loop fusion | flops 3145728 | bytes 9437184 | tf_op jit(solution)/shard_map/mul | solution.py:416
  248.2 0.0 copy-done.5
  248.2 0.0 copy-start.9
  248.2 2.1 convert_multiply_fusion
  250.3 0.0 copy-done.9
  250.3 0.6 copy.18
  (2 shorter events, 0.0 us)
Async XLA Ops:
  86.2 8.6 %copy-start.6 = (bf16[8,256,384]{2,1,0:T(8,128)(2,1)S(1)}, bf16[8,256,384]{2,1,0:T(8,128)(2,1)}, u32[]{:S(2)}) copy-start(bf16[8,256,384]{2,1,0:T(8,128)(2,1)} %get-tuple-element.15) | copy-start | bytes 4718596
  86.2 8.6 %copy-start.10 = (bf16[8,256,2048]{2,1,0:T(8,128)(2,1)S(1)}, bf16[8,256,2048]{2,1,0:T(8,128)(2,1)}, u32[]{:S(2)}) copy-start(bf16[8,256,2048]{2,1,0:T(8,128)(2,1)} %get-tuple-element.19) | copy-start | bytes 25165828
  94.8 5.6 %copy-start.7 = (bf16[8,256,384]{2,1,0:T(8,128)(2,1)S(1)}, bf16[8,256,384]{2,1,0:T(8,128)(2,1)}, u32[]{:S(2)}) copy-start(bf16[8,256,384]{2,1,0:T(8,128)(2,1)} %get-tuple-element.16) | copy-start | bytes 4718596
  106.1 134.1 %copy-start = (bf16[256,2048]{1,0:T(8,128)(2,1)S(1)}, bf16[256,2048]{1,0:T(8,128)(2,1)}, u32[]{:S(2)}) copy-start(bf16[256,2048]{1,0:T(8,128)(2,1)} %refs_0_.1) | copy-start | bytes 3145732
  106.1 134.5 %copy-start.8 = (f32[2048]{0:T(1024)S(1)}, f32[2048]{0:T(1024)}, u32[]{:S(2)}) copy-start(f32[2048]{0:T(1024)} %param.7) | copy-start | bytes 24580
  240.2 2.6 %copy-start.1 = (f32[256,2048]{1,0:T(8,128)S(1)}, f32[256,2048]{1,0:T(8,128)}, u32[]{:S(2)}) copy-start(f32[256,2048]{1,0:T(8,128)} %get-tuple-element.20) | copy-start | bytes 6291460
  240.3 2.6 %copy-start.2 = (bf16[256,2048]{1,0:T(8,128)(2,1)S(1)}, bf16[256,2048]{1,0:T(8,128)(2,1)}, u32[]{:S(2)}) copy-start(bf16[256,2048]{1,0:T(8,128)(2,1)} %g_ref.1) | copy-start | bytes 3145732
  242.8 1.8 copy-start.3
  242.8 2.1 copy-start.4
  245.0 3.3 %copy-start.5 = (bf16[384,2048]{1,0:T(8,128)(2,1)S(1)}, bf16[384,2048]{1,0:T(8,128)(2,1)}, u32[]{:S(2)}) copy-start(bf16[384,2048]{1,0:T(8,128)(2,1)} %get-tuple-element.24) | copy-start | bytes 4718596
  248.2 2.1 copy-start.9
